TPU v7x, 32 devices: a whole 2x2x4 slice. The times are simulated.
32 devices in a mesh: sp: 8 (over z, x), tp: 4 (over y, core).
Axes of the slice: x: 2, y: 2, z: 4, core: 2. Of those that a mesh axis runs over, the one named last changes fastest.
Arguments:
- upstream: bfloat16 [2048, 2048], P('sp'), may hold values from -6 to 6
- stream: bfloat16 [2048, 2048], P('sp'), may hold values from -10 to 10
- routes: int32 [2048, 2], P('sp'), may hold values from 0 to 7, all different within a row; in each aligned block of 256 rows (0 to 255, 256 to 511, ...) at most 128 rows name the same one
- route_weights: float32 [2048, 2], P('sp'), may hold values from 0.1 to 1
- glu_value: bfloat16 [2048, 512], P('sp', 'tp'), may hold values from -6 to 6
- glu_gate: bfloat16 [2048, 512], P('sp', 'tp'), may hold values from -10 to 10
- conv_taps: float32 [31, 512], P(None, 'tp'), may hold values from -1 to 1
- conv_saved: bfloat16 [2048, 512], P('sp', 'tp'), may hold values from -600 to 600
- out_proj: bfloat16 [2048, 512], P(None, 'tp'), may hold values from -0.25 to 0.25
- expert_gate: bfloat16 [8, 2048, 2048], P('sp', None, 'tp'), may hold values from -0.125 to 0.125
- expert_up: bfloat16 [8, 2048, 2048], P('sp', None, 'tp'), may hold values from -0.125 to 0.125
- expert_down: bfloat16 [8, 2048, 2048], P('sp', 'tp'), may hold values from -0.125 to 0.125
Outputs:
- grad_stream: bfloat16 [2048, 2048], P('sp', 'tp')
- grad_value: bfloat16 [2048, 512], P('sp', 'tp')
- grad_gate: bfloat16 [2048, 512], P('sp', 'tp')
- grad_out_proj: float32 [2048, 512], P('sp', 'tp')
- grad_expert_gate: float32 [8, 2048, 2048], P('sp', None, 'tp')
- grad_expert_up: float32 [8, 2048, 2048], P('sp', None, 'tp')
- grad_expert_down: float32 [8, 2048, 2048], P('sp', 'tp')
Inputs may be any that keep to these rules, and one draw needn't show every extreme that they name: `routes`: each row names 2 different experts; among the 256 rows of one index of sp no expert is named more than 128 times, a bound that some block reaches.
All inputs are finite; a program needn't handle non-finite values.
Results may differ from a plain program's by a relative error of at most 0.014.
Values may be sent and summed in bfloat16 or wider, within the bound.
A program may use at most 128 MiB of HBM per device.

v0:
```python
import jax
import jax.numpy as jnp
from jax import lax
from jax.sharding import PartitionSpec as P

clamp_limit = 7.0
glu_alpha = 1.702
norm_eps = 1e-05


def passed_along(shard, axis, by):
    size = lax.axis_size(axis)
    pairs = [(i, i + by) for i in range(size) if 0 <= i + by < size]
    return lax.ppermute(shard, axis, pairs)


def contract_rows(left, right):
    return lax.dot_general(
        left, right, (((0,), (0,)), ((), ())), preferred_element_type=jnp.float32
    )


def times_transposed(left, right):
    return lax.dot_general(
        left, right, (((1,), (1,)), ((), ())), preferred_element_type=jnp.float32
    )


def pair_rows(block_routes, expert_count, capacity):
    tok_count, topk = block_routes.shape
    experts = jnp.arange(expert_count, dtype=jnp.int32)[None, :]
    hots = [(block_routes[:, k : k + 1] == experts).astype(jnp.float32) for k in range(topk)]
    before = (jnp.arange(tok_count)[:, None] > jnp.arange(tok_count)[None, :]).astype(jnp.bfloat16)
    earlier = jnp.dot(before, sum(hots).astype(jnp.bfloat16), preferred_element_type=jnp.float32)
    slots = [jnp.sum(earlier * hot, axis=1).astype(jnp.int32) for hot in hots]
    return [block_routes[:, k] * capacity + slots[k] for k in range(topk)]


def select_pairs(targets, block_weights, row_count):
    rows = jnp.arange(row_count, dtype=jnp.int32)[:, None]
    hits = [target[None, :] == rows for target in targets]
    picks = sum((hit.astype(jnp.float32) for hit in hits)).astype(jnp.bfloat16)
    row_weights = jnp.sum(
        sum((jnp.where(hit, block_weights[:, k][None, :], 0.0) for k, hit in enumerate(hits))),
        axis=1,
    )
    return (picks, row_weights)


def expert_backward(expert_rows, expert_cot, gate_weight, up_weight, down_weight):
    gate_pre = jnp.dot(expert_rows, gate_weight, preferred_element_type=jnp.float32)
    up_pre = jnp.dot(expert_rows, up_weight, preferred_element_type=jnp.float32)
    capped = jnp.minimum(gate_pre, clamp_limit)
    clipped = jnp.clip(up_pre, -clamp_limit, clamp_limit)
    gate_sigmoid = jax.nn.sigmoid(glu_alpha * capped)
    act = (capped * gate_sigmoid * (clipped + 1.0)).astype(jnp.bfloat16)
    grad_down = contract_rows(act, expert_cot)
    grad_act = times_transposed(expert_cot, down_weight)
    slope = gate_sigmoid + glu_alpha * capped * gate_sigmoid * (1.0 - gate_sigmoid)
    grad_gate_pre = jnp.where(
        gate_pre < clamp_limit, grad_act * (clipped + 1.0) * slope, 0.0
    ).astype(jnp.bfloat16)
    grad_up_pre = jnp.where(
        jnp.abs(up_pre) < clamp_limit, grad_act * capped * gate_sigmoid, 0.0
    ).astype(jnp.bfloat16)
    grad_gate = contract_rows(expert_rows, grad_gate_pre)
    grad_up = contract_rows(expert_rows, grad_up_pre)
    return (grad_gate, grad_up, grad_down, grad_gate_pre, grad_up_pre)


def on_device(
    upstream,
    stream,
    routes,
    route_weights,
    glu_value,
    glu_gate,
    conv_taps,
    conv_saved,
    out_proj,
    expert_gate,
    expert_up,
    expert_down,
):
    tok_count = upstream.shape[0]
    model_width = upstream.shape[1]
    expert_count = lax.axis_size("sp")
    capacity = 4 * tok_count // expert_count
    slice_width = model_width // lax.axis_size("tp")
    column_start = lax.axis_index("tp") * slice_width
    targets = pair_rows(routes, expert_count, capacity)
    picks, row_weights = select_pairs(targets, route_weights, expert_count * capacity)
    stream_part = lax.dynamic_slice_in_dim(stream, column_start, slice_width, 1)
    upstream_part = lax.dynamic_slice_in_dim(upstream, column_start, slice_width, 1)
    send_rows = jnp.dot(picks, stream_part, preferred_element_type=jnp.float32).astype(jnp.bfloat16)
    send_cot = (
        row_weights[:, None] * jnp.dot(picks, upstream_part, preferred_element_type=jnp.float32)
    ).astype(jnp.bfloat16)
    part_shape = (expert_count, capacity, slice_width)
    part_rows, part_cot = (
        lax.all_to_all(
            send_rows.reshape(part_shape), "sp", split_axis=0, concat_axis=0, tiled=True
        ),
        lax.all_to_all(send_cot.reshape(part_shape), "sp", split_axis=0, concat_axis=0, tiled=True),
    )
    got_rows, got_cot = (
        lax.all_gather(part_rows, "tp", axis=2, tiled=True),
        lax.all_gather(part_cot, "tp", axis=2, tiled=True),
    )
    expert_rows = got_rows.reshape(-1, model_width)
    expert_cot = got_cot.reshape(-1, model_width)
    gate_weight = expert_gate[0]
    up_weight = expert_up[0]
    down_weight = expert_down[0]
    grad_gate_w, grad_up_w, grad_down_w, grad_gate_pre, grad_up_pre = expert_backward(
        expert_rows, expert_cot, gate_weight, up_weight, down_weight
    )
    partial_rows = times_transposed(grad_gate_pre, gate_weight) + times_transposed(
        grad_up_pre, up_weight
    )
    summed_rows = lax.psum_scatter(
        partial_rows.astype(jnp.bfloat16), "tp", scatter_dimension=1, tiled=True
    )
    returned = lax.all_to_all(
        summed_rows.reshape(expert_count, capacity, slice_width),
        "sp",
        split_axis=0,
        concat_axis=0,
        tiled=True,
    )
    routed_sum = contract_rows(picks, returned.reshape(expert_count * capacity, slice_width))
    upstream_own = lax.dynamic_slice_in_dim(upstream, column_start, slice_width, 1)
    grad_stream = (upstream_own.astype(jnp.float32) + routed_sum).astype(jnp.bfloat16)
    full_grad = lax.all_gather(grad_stream, "tp", axis=1, tiled=True)
    conv_width = conv_saved.shape[1] * lax.axis_size("tp")
    saved_conv = conv_saved.astype(jnp.float32)
    total_sum, square_sum = lax.psum(
        (jnp.sum(saved_conv, axis=1), jnp.sum(saved_conv * saved_conv, axis=1)), "tp"
    )
    mean_c = (total_sum / conv_width)[:, None]
    var_c = (square_sum / conv_width)[:, None] - mean_c * mean_c
    inv_std = lax.rsqrt(var_c + norm_eps)
    normed = (saved_conv - mean_c) * inv_std
    norm_sigmoid = jax.nn.sigmoid(normed)
    mixed = (normed * norm_sigmoid).astype(jnp.bfloat16)
    grad_mixed = jnp.dot(full_grad, out_proj, preferred_element_type=jnp.float32)
    grad_normed = grad_mixed * norm_sigmoid * (1.0 + normed * (1.0 - norm_sigmoid))
    first_sum, second_sum = lax.psum(
        (jnp.sum(grad_normed, axis=1), jnp.sum(grad_normed * normed, axis=1)), "tp"
    )
    grad_conv = inv_std * (
        grad_normed
        - (first_sum / conv_width)[:, None]
        - normed * (second_sum / conv_width)[:, None]
    )
    kernel_width = conv_taps.shape[0]
    rim_rows = passed_along(grad_conv[: kernel_width - 1], "sp", -1)
    padded = jnp.concatenate([grad_conv, rim_rows], axis=0)
    grad_glu = jnp.zeros_like(grad_conv)
    for offset in range(kernel_width):
        grad_glu = grad_glu + conv_taps[offset][None, :] * padded[offset : offset + tok_count]
    gate_sig = jax.nn.sigmoid(glu_gate.astype(jnp.float32))
    grad_value = (grad_glu * gate_sig).astype(jnp.bfloat16)
    grad_gate = (grad_glu * glu_value.astype(jnp.float32) * gate_sig * (1.0 - gate_sig)).astype(
        jnp.bfloat16
    )
    proj_parts = contract_rows(full_grad, mixed).astype(jnp.bfloat16)
    proj_parts = lax.all_to_all(
        proj_parts.reshape(expert_count, -1, mixed.shape[1]),
        "sp",
        split_axis=0,
        concat_axis=0,
        tiled=True,
    )
    grad_out_proj = jnp.sum(proj_parts.astype(jnp.float32), axis=0)
    return (
        grad_stream,
        grad_value,
        grad_gate,
        grad_out_proj,
        grad_gate_w[None],
        grad_up_w[None],
        grad_down_w[None],
    )


def solution(mesh):
    in_specs = (
        P("sp", None),
        P("sp", None),
        P("sp", None),
        P("sp", None),
        P("sp", "tp"),
        P("sp", "tp"),
        P(None, "tp"),
        P("sp", "tp"),
        P(None, "tp"),
        P("sp", None, "tp"),
        P("sp", None, "tp"),
        P("sp", "tp", None),
    )
    out_specs = (
        P("sp", "tp"),
        P("sp", "tp"),
        P("sp", "tp"),
        P("sp", "tp"),
        P("sp", None, "tp"),
        P("sp", None, "tp"),
        P("sp", "tp", None),
    )
    return jax.shard_map(
        on_device, mesh=mesh, in_specs=in_specs, out_specs=out_specs, check_vma=False
    )
```

profile of v0, /device:TPU:0, one launch (start us, length us, event | category | flops | bytes accessed | tf_op | source)
XLA Modules:
  0.0 257.4 jit_solution(7277678649317412577)
XLA Ops:
  7.2 0.0 copy-start
  7.2 0.0 all-gather.4.cloned.1.call-start
  7.2 0.8 fusion.143
  8.1 0.2 select_reduce_fusion.1
  8.3 0.0 copy-start.5
  8.3 1.4 convolution_convert_fusion.1
  9.7 32.9 %all_to_all.20 = bf16[8,128,512]{2,1,0:T(8,128)(2,1)} all-to-all(bf16[8,128,512]{2,1,0:T(8,128)(2,1)S(1)} %bitcast.111), channel_id=1, replica_groups=mesh['sp'=8,'tp'=4] {'sp'}, dimensions={0} | all-to-all | bytes 2097152 | tf_op jit(solution)/shard_map/all_to_all | solution.py:101
  42.7 0.0 all-gather.4.cloned.1.call-update
  42.7 0.0 all-gather.6.cloned.1.call-start
  42.7 0.0 copy-done.5
  42.8 0.3 add_reduce_fusion
  43.1 1.4 multiply_convert_fusion.1
  44.5 29.0 %all_to_all.21 = bf16[8,128,512]{2,1,0:T(8,128)(2,1)} all-to-all(bf16[8,128,512]{2,1,0:T(8,128)(2,1)S(1)} %bitcast.110), channel_id=1, replica_groups=mesh['sp'=8,'tp'=4] {'sp'}, dimensions={0} | all-to-all | bytes 2097152 | tf_op jit(solution)/shard_map/all_to_all | solution.py:104
  73.4 0.0 all-gather.6.cloned.1.call-update
  73.5 0.0 reduce-scatter.2.cloned.1.call-start
  73.5 2.8 %all-gather.4.cloned.1.call-done = bf16[8,128,2048]{2,1,0:T(8,128)(2,1)} async-done(((bf16[8,128,512]{2,1,0:T(8,128)(2,1)}), bf16[8,128,2048]{2,1,0:T(8,128)(2,1)}) %all-gather.4.cloned.1.call-update) | async-done | bytes 4194320 | tf_op jit(solution)/shard_map/all_gather | solution.py:107
  76.3 6.6 %fusion.1 = f32[1024,512]{1,0:T(8,128)} fusion(bf16[1024,2048]{1,0:T(8,128)(2,1)} %bitcast.118, bf16[1,2048,512]{2,1,0:T(8,128)(2,1)} %param.22), kind=kOutput, calls=%fused_computation.6 | convolution fusion | flops 2147483648 | bytes 8388608 | tf_op jit(solution)/shard_map/dot_general | solution.py:52
  83.0 0.0 copy-done
  83.0 0.0 copy-done.6
  83.0 3.7 %fusion.7 = f32[1024,512]{1,0:T(8,128)} fusion(bf16[1024,2048]{1,0:T(8,128)(2,1)S(1)} %bitcast.121, bf16[1,2048,512]{2,1,0:T(8,128)(2,1)S(1)} %copy-done), kind=kOutput, calls=%fused_computation.12 | convolution fusion | flops 2147483648 | bytes 8388608 | tf_op jit(solution)/shard_map/dot_general | solution.py:51
  86.7 25.7 %all-gather.6.cloned.1.call-done = bf16[8,128,2048]{2,1,0:T(8,128)(2,1)} async-done(((bf16[8,128,512]{2,1,0:T(8,128)(2,1)}), bf16[8,128,2048]{2,1,0:T(8,128)(2,1)}) %all-gather.6.cloned.1.call-update) | async-done | bytes 4194320 | tf_op jit(solution)/shard_map/all_gather | solution.py:108
  112.4 7.6 %select_convert_fusion = (bf16[1024,512]{1,0:T(8,128)(2,1)S(1)}, bf16[1024,512]{1,0:T(8,128)(2,1)S(1)}) fusion(f32[1024,512]{1,0:T(8,128)} %fusion.1, f32[1024,512]{1,0:T(8,128)} %fusion.7, bf16[1024,2048]{1,0:T(8,128)(2,1)} %bitcast.122, bf16[1,512,2048]{2,1,0:T(8,128)(2,1)} %param.23), kind=kOutput, calls=%fused_computation.15 | convolution fusion | flops 2159017984 | bytes 12582912 | tf_op jit(solution)/shard_map/dot_general | solution.py:24
  120.0 0.0 copy-start.11
  120.0 0.0 copy-start.10
  120.0 0.0 copy-start.8
  120.1 2.4 fusion.5
  122.4 0.0 copy-done.11
  122.4 0.0 copy-done.10
  122.5 0.0 copy-done.8
  122.5 4.4 %add_convert_fusion = bf16[1024,2048]{1,0:T(8,128)(2,1)} fusion(f32[1024,2048]{1,0:T(8,128)S(1)} %fusion.5, bf16[1024,512]{1,0:T(8,128)(2,1)S(1)} %get-tuple-element.19, bf16[1,2048,512]{2,1,0:T(8,128)(2,1)S(1)} %copy-done.8), kind=kOutput, calls=%fused_computation | convolution fusion | flops 2151677952 | bytes 15728640 | tf_op jit(solution)/shard_map/dot_general | solution.py:24
  126.9 0.0 reduce-scatter.2.cloned.1.call-update
  126.9 0.0 copy-start.2
  126.9 0.0 copy-start.4
  126.9 44.5 %reduce-scatter.2.cloned.1.call-done = bf16[1024,512]{1,0:T(8,128)(2,1)} async-done(((bf16[1024,2048]{1,0:T(8,128)(2,1)}), bf16[1024,512]{1,0:T(8,128)(2,1)}) %reduce-scatter.2.cloned.1.call-update) | async-done | bytes 1048592 | tf_op jit(solution)/shard_map/reduce_scatter | solution.py:121
  171.4 5.7 %all-to-all-start.2 = ((bf16[8,128,512]{2,1,0:T(8,128)(2,1)}), bf16[8,128,512]{2,1,0:T(8,128)(2,1)S(1)}, u32[]{:S(2)}, u32[]{:S(2)}) async-start(bf16[8,128,512]{2,1,0:T(8,128)(2,1)} %bitcast.108), calls=%async_computation.3 | async-start | bytes 2097152 | tf_op jit(solution)/shard_map/all_to_all | solution.py:124
  177.1 0.0 all-gather.8.cloned.1.call-start
  177.2 0.0 copy-done.2
  177.2 0.1 fusion.112
  177.3 6.0 %all-reduce.1 = (f32[256]{0:T(256)S(1)}, f32[256]{0:T(256)S(1)}) all-reduce(f32[256]{0:T(256)S(1)} %get-tuple-element.10, f32[256]{0:T(256)S(1)} %get-tuple-element.9), channel_id=1, replica_groups=mesh['sp'=8,'tp'=4] {'tp'}, use_global_device_ids=true, to_apply=%region_7.8 | all-reduce | flops 512 | bytes 4096 | tf_op jit(solution)/shard_map/psum | solution.py:137
  183.3 0.0 copy-done.4
  183.3 19.5 %all-to-all-done.2 = bf16[8,128,512]{2,1,0:T(8,128)(2,1)S(1)} async-done(((bf16[8,128,512]{2,1,0:T(8,128)(2,1)}), bf16[8,128,512]{2,1,0:T(8,128)(2,1)S(1)}, u32[]{:S(2)}, u32[]{:S(2)}) %all-to-all-start.2) | async-done | bytes 1048608 | tf_op jit(solution)/shard_map/all_to_all | solution.py:124
  202.8 2.1 fusion.9
  204.9 0.0 all-gather.8.cloned.1.call-update
  205.0 0.0 copy-start.7
  205.0 0.0 copy-start.12
  205.0 7.0 %convolution_bitcast_fusion.1 = f32[1,2048,512]{2,1,0:T(8,128)} fusion(bf16[1024,2048]{1,0:T(8,128)(2,1)} %bitcast.119, bf16[1024,512]{1,0:T(8,128)(2,1)} %copy-done.10), kind=kOutput, calls=%fused_computation.2 | convolution fusion | flops 2147483648 | bytes 9437184 | tf_op jit(solution)/shard_map/dot_general | solution.py:18
  212.0 0.0 copy-done.12
  212.0 0.0 copy-start.9
  212.1 4.8 %convolution_bitcast_fusion = f32[1,512,2048]{2,1,0:T(8,128)} fusion(bf16[1024,2048]{1,0:T(8,128)(2,1)S(1)} %bitcast.123, f32[1024,512]{1,0:T(8,128)S(1)} %copy-done.13, f32[1024,512]{1,0:T(8,128)S(1)} %copy-done.12), kind=kOutput, calls=%fused_computation.1 | convolution fusion | flops 2152726528 | bytes 12582912 | tf_op jit(solution)/shard_map/dot_general | solution.py:18
  216.9 3.0 %all-gather.8.cloned.1.call-done = bf16[256,2048]{1,0:T(8,128)(2,1)} async-done(((bf16[256,512]{1,0:T(8,128)(2,1)}), bf16[256,2048]{1,0:T(8,128)(2,1)}) %all-gather.8.cloned.1.call-update) | async-done | bytes 1048592 | tf_op jit(solution)/shard_map/all_gather | solution.py:134
  219.8 1.8 fusion.141
  221.6 5.9 %all-reduce = (f32[256]{0:T(256)S(1)}, f32[256]{0:T(256)S(1)}) all-reduce(f32[256]{0:T(256)S(1)} %get-tuple-element.8, f32[256]{0:T(256)S(1)} %get-tuple-element.7), channel_id=1, replica_groups=mesh['sp'=8,'tp'=4] {'tp'}, use_global_device_ids=true, to_apply=%region_11.12 | all-reduce | flops 512 | bytes 4096 | tf_op jit(solution)/shard_map/psum | solution.py:148
  227.5 2.6 %convolution_convert_fusion = bf16[2048,128]{1,0:T(8,128)(2,1)} fusion(bf16[256,2048]{1,0:T(8,128)(2,1)} %all-gather.8.cloned.1.call-done, bf16[256,128]{1,0:T(8,128)(2,1)S(1)} %copy-done.2, f32[256]{0:T(256)S(1)} %get-tuple-element.57, f32[256]{0:T(256)S(1)} %get-tuple-element.56), kind=kOutput, calls=%fused_computation.4 | convolution fusion | flops 134742016 | bytes 1640448 | tf_op jit(solution)/shard_map/dot_general | solution.py:18
  230.1 5.7 %all-to-all-start.3 = ((bf16[8,256,128]{2,1,0:T(8,128)(2,1)}), bf16[8,256,128]{2,1,0:T(8,128)(2,1)S(1)}, u32[]{:S(2)}, u32[]{:S(2)}) async-start(bf16[8,256,128]{2,1,0:T(8,128)(2,1)} %bitcast.44), calls=%async_computation.4 | async-start | bytes 1048576 | tf_op jit(solution)/shard_map/all_to_all | solution.py:168
  235.8 0.2 fusion.125
  236.0 0.0 copy-start.1
  236.0 0.0 copy-start.3
  236.0 1.4 collective-permute-start
  237.4 6.9 %convolution_bitcast_fusion.2 = f32[1,2048,512]{2,1,0:T(8,128)} fusion(bf16[1024,2048]{1,0:T(8,128)(2,1)} %bitcast.120, bf16[1024,512]{1,0:T(8,128)(2,1)} %copy-done.11), kind=kOutput, calls=%fused_computation.3 | convolution fusion | flops 2147483648 | bytes 9437184 | tf_op jit(solution)/shard_map/dot_general | solution.py:18
  244.3 0.0 collective-permute-done
  244.3 1.1 multiply_convert_fusion.3
  245.4 0.7 multiply_convert_fusion.4
  246.1 4.1 %all-to-all-done.3 = bf16[8,256,128]{2,1,0:T(8,128)(2,1)S(1)} async-done(((bf16[8,256,128]{2,1,0:T(8,128)(2,1)}), bf16[8,256,128]{2,1,0:T(8,128)(2,1)S(1)}, u32[]{:S(2)}, u32[]{:S(2)}) %all-to-all-start.3) | async-done | bytes 524320 | tf_op jit(solution)/shard_map/all_to_all | solution.py:168
  250.1 0.7 convert_reduce_fusion
  (15 shorter events, 0.1 us)
Async XLA Ops:
  7.2 75.8 %copy-start = (bf16[1,2048,512]{2,1,0:T(8,128)(2,1)S(1)}, bf16[1,2048,512]{2,1,0:T(8,128)(2,1)}, u32[]{:S(2)}) copy-start(bf16[1,2048,512]{2,1,0:T(8,128)(2,1)} %param.21) | copy-start | bytes 6291460
  7.2 69.2 %all-gather.4.cloned.1.call-start = ((), (), s32[]{:S(2)}) async-start(), calls=%async_computation.5 | async-start | bytes 5242880 | tf_op jit(solution)/shard_map/all_gather | solution.py:107
  8.3 34.5 %copy-start.5 = (f32[256,2]{0,1:T(2,128)S(1)}, f32[256,2]{0,1:T(2,128)}, u32[]{:S(2)}) copy-start(f32[256,2]{0,1:T(2,128)} %param.15) | copy-start | bytes 6148
  42.7 69.7 %all-gather.6.cloned.1.call-start = ((), (), s32[]{:S(2)}) async-start(), calls=%async_computation.6 | async-start | bytes 5242880 | tf_op jit(solution)/shard_map/all_gather | solution.py:108
  73.5 98.0 %reduce-scatter.2.cloned.1.call-start = ((), (), s32[]{:S(2)}) async-start(), calls=%async_computation.7 | async-start | bytes 5242880 | tf_op jit(solution)/shard_map/reduce_scatter | solution.py:121
  76.3 6.6 %copy-start.6 = (bf16[8,128,2048]{2,1,0:T(8,128)(2,1)S(1)}, bf16[8,128,2048]{2,1,0:T(8,128)(2,1)}, u32[]{:S(2)}) copy-start(bf16[8,128,2048]{2,1,0:T(8,128)(2,1)} %all-gather.4.cloned.1.call-done) | copy-start | bytes 12582916
  120.0 2.4 copy-start.11
  120.0 2.4 copy-start.10
  120.0 2.4 copy-start.8
  126.9 50.3 %copy-start.2 = (bf16[256,128]{1,0:T(8,128)(2,1)S(1)}, bf16[256,128]{1,0:T(8,128)(2,1)}, u32[]{:S(2)}) copy-start(bf16[256,128]{1,0:T(8,128)(2,1)} %param.19) | copy-start | bytes 196612
  126.9 56.4 %copy-start.4 = (f32[31,128]{1,0:T(8,128)S(1)}, f32[31,128]{1,0:T(8,128)}, u32[]{:S(2)}) copy-start(f32[31,128]{1,0:T(8,128)} %param.18) | copy-start | bytes 47620
  171.4 31.4 %all-to-all-start.2 = ((bf16[8,128,512]{2,1,0:T(8,128)(2,1)}), bf16[8,128,512]{2,1,0:T(8,128)(2,1)S(1)}, u32[]{:S(2)}, u32[]{:S(2)}) async-start(bf16[8,128,512]{2,1,0:T(8,128)(2,1)} %bitcast.108), calls=%async_computation.3 | async-start | bytes 2097152 | tf_op jit(solution)/shard_map/all_to_all | solution.py:124
  177.1 42.7 %all-gather.8.cloned.1.call-start = ((), (), s32[]{:S(2)}) async-start(), calls=%async_computation.8 | async-start | bytes 1310720 | tf_op jit(solution)/shard_map/all_gather | solution.py:134
  205.0 7.1 %copy-start.7 = (bf16[8,128,2048]{2,1,0:T(8,128)(2,1)S(1)}, bf16[8,128,2048]{2,1,0:T(8,128)(2,1)}, u32[]{:S(2)}) copy-start(bf16[8,128,2048]{2,1,0:T(8,128)(2,1)} %all-gather.6.cloned.1.call-done) | copy-start | bytes 12582916
  205.0 7.1 %copy-start.12 = (f32[1024,512]{1,0:T(8,128)S(1)}, f32[1024,512]{1,0:T(8,128)}, u32[]{:S(2)}) copy-start(f32[1024,512]{1,0:T(8,128)} %fusion.1) | copy-start | bytes 6291460
  205.0 7.0 %copy-start.13 = (f32[1024,512]{1,0:T(8,128)S(1)}, f32[1024,512]{1,0:T(8,128)}, u32[]{:S(2)}) copy-start(f32[1024,512]{1,0:T(8,128)} %fusion.7) | copy-start | bytes 6291460
  212.0 7.8 %copy-start.9 = (bf16[2048,128]{1,0:T(8,128)(2,1)S(1)}, bf16[2048,128]{1,0:T(8,128)(2,1)}, u32[]{:S(2)}) copy-start(bf16[2048,128]{1,0:T(8,128)(2,1)} %param.20) | copy-start | bytes 1572868
  230.1 20.0 %all-to-all-start.3 = ((bf16[8,256,128]{2,1,0:T(8,128)(2,1)}), bf16[8,256,128]{2,1,0:T(8,128)(2,1)S(1)}, u32[]{:S(2)}, u32[]{:S(2)}) async-start(bf16[8,256,128]{2,1,0:T(8,128)(2,1)} %bitcast.44), calls=%async_computation.4 | async-start | bytes 1048576 | tf_op jit(solution)/shard_map/all_to_all | solution.py:168
  236.0 8.3 %copy-start.1 = (bf16[256,128]{1,0:T(8,128)(2,1)S(1)}, bf16[256,128]{1,0:T(8,128)(2,1)}, u32[]{:S(2)}) copy-start(bf16[256,128]{1,0:T(8,128)(2,1)} %param.17) | copy-start | bytes 196612
  236.0 8.3 %copy-start.3 = (bf16[256,128]{1,0:T(8,128)(2,1)S(1)}, bf16[256,128]{1,0:T(8,128)(2,1)}, u32[]{:S(2)}) copy-start(bf16[256,128]{1,0:T(8,128)(2,1)} %param.16) | copy-start | bytes 196612
  236.0 8.3 %collective-permute-start = (f32[30,128]{1,0:T(8,128)S(1)}, f32[30,128]{1,0:T(8,128)S(1)}, u32[]{:S(2)}, u32[]{:S(2)}) collective-permute-start(f32[30,128]{1,0:T(8,128)S(1)} %slice.266), channel_id=1, source_target_pairs={{4,0},{8,4},{12,8},{16,12},{20,16},{24,20},{28,24},{5,1},{9,5},{13... | collective-permute-start | bytes 46088 | tf_op jit(solution)/shard_map/ppermute | solution.py:14
Sparse Core Ops, SparseCore 0:
  42.8 33.4 all-gather.3
  77.9 34.4 all-gather.5
  127.0 44.3 reduce-scatter.1
  205.1 14.7 all-gather.7
where the time goes:
time: 258 us; the launch traced here: 257 us
  waiting for transfers between devices  99.6 us (39%)
  blocking collectives  73.8 us (29%)
  matrix products  53 us (21%)
  between operations  14 us (5%)
  starting transfers between devices  12.9 us (5%)
  other arithmetic  3.14 us (1%)
    reduce_scatter x1, waiting for transfers between devices, on_device(): lax.psum_scatter(partial_rows.astype(jnp.bfloat16), 'tp', scatter_dimensi...  44.5 us
    all_to_all x1, blocking collectives, on_device(): lax.all_to_all(send_rows.reshape(part_shape), 'sp', split_axis=0, concat_...  32.9 us
    all_to_all x1, blocking collectives, on_device(): lax.all_to_all(send_cot.reshape(part_shape), 'sp', split_axis=0, concat_a...  29 us
    all_gather x1, waiting for transfers between devices, on_device(): lax.all_gather(part_cot, 'tp', axis=2, tiled=True)  25.7 us
    dot_general x5, matrix products, contract_rows(): lax.dot_general(left, right, (((0,), (0,)), ((), ())), preferred_element_...  23.4 us
    all_to_all x1, waiting for transfers between devices, on_device(): lax.all_to_all(summed_rows.reshape(expert_count, capacity, slice_width),...  19.5 us
    dot_general x3, matrix products, times_transposed(): lax.dot_general(left, right, (((1,), (1,)), ((), ())), preferred_element_...  14.4 us
    dot_general x1, matrix products, expert_backward(): up_pre = jnp.dot(expert_rows, up_weight, preferred_element_type=jnp.float32)  6.64 us
  transfers between devices with their start and end apart: 7, of which 6 were waited for; matrix products, arithmetic and copies ran while one was open for 13% of the time, Pallas kernels for 0%

commit v1 on v0

--- a/solution.py
+++ b/solution.py
@@ -105,7 +105,9 @@
     )
     got_rows, got_cot = (
         lax.all_gather(part_rows, "tp", axis=2, tiled=True),
-        lax.all_gather(part_cot, "tp", axis=2, tiled=True),
+        jnp.concatenate(
+            lax.all_to_all(jnp.stack([part_cot] * lax.axis_size("tp")), "tp", 0, 0), axis=2
+        ),
     )
     expert_rows = got_rows.reshape(-1, model_width)
     expert_cot = got_cot.reshape(-1, model_width)

time: 258 us -> 274 us (1.062)
  starting transfers between devices: 12.9 us -> 17.7 us
  waiting for transfers between devices: 99.6 us -> 104 us
  local copies, waits for them, and re-layouts: 0.95 us -> 5.21 us
    all_to_all x0 -> x1, waiting for transfers between devices: none -> 37.6 us  [on_device(): lax.all_to_all(jnp.stack([part_cot] * lax.axis_size('tp')), 'tp', 0, 0)]
    all_gather x1 -> x0, waiting for transfers between devices: 25.7 us -> none  [on_device(): lax.all_gather(part_cot, 'tp', axis=2, tiled=True)]
    all_to_all x0 -> x1, starting transfers between devices: none -> 4.83 us  [on_device(): lax.all_to_all(jnp.stack([part_cot] * lax.axis_size('tp')), 'tp', 0, 0)]
    all_gather x1, waiting for transfers between devices: 2.83 us -> 0.02 us  [on_device(): lax.all_gather(part_rows, 'tp', axis=2, tiled=True)]
  transfers between devices with their start and end apart: 7 -> 7, of which waited for: 6 -> 5; matrix products, arithmetic and copies ran while one was open for 13% -> 14% of each run, Pallas kernels for 0% -> 0%
where the time goes in v1:
time: 274 us
  waiting for transfers between devices  104 us (38%)
  blocking collectives  74 us (27%)
  matrix products  55.6 us (20%)
  starting transfers between devices  17.7 us (6%)
  between operations  14 us (5%)
  local copies, waits for them, and re-layouts  5.21 us (2%)
  other arithmetic  3.14 us (1%)
    reduce_scatter x1, waiting for transfers between devices, on_device(): lax.psum_scatter(partial_rows.astype(jnp.bfloat16), 'tp', scatter_dimensi...  42.6 us
    all_to_all x1, waiting for transfers between devices, on_device(): lax.all_to_all(jnp.stack([part_cot] * lax.axis_size('tp')), 'tp', 0, 0)  37.6 us
    all_to_all x1, blocking collectives, on_device(): lax.all_to_all(send_rows.reshape(part_shape), 'sp', split_axis=0, concat_...  32.9 us
    all_to_all x1, blocking collectives, on_device(): lax.all_to_all(send_cot.reshape(part_shape), 'sp', split_axis=0, concat_a...  29 us
    dot_general x5, matrix products, contract_rows(): lax.dot_general(left, right, (((0,), (0,)), ((), ())), preferred_element_...  26 us
    all_to_all x1, waiting for transfers between devices, on_device(): lax.all_to_all(summed_rows.reshape(expert_count, capacity, slice_width),...  19.2 us
    dot_general x3, matrix products, times_transposed(): lax.dot_general(left, right, (((1,), (1,)), ((), ())), preferred_element_...  14.5 us
    dot_general x1, matrix products, expert_backward(): up_pre = jnp.dot(expert_rows, up_weight, preferred_element_type=jnp.float32)  6.65 us
  transfers between devices with their start and end apart: 7, of which 5 were waited for; matrix products, arithmetic and copies ran while one was open for 14% of the time, Pallas kernels for 0%

profile of v1, /device:TPU:0, one launch (start us, length us, event | category | flops | bytes accessed | tf_op | source)
XLA Modules:
  0.0 273.7 jit_solution(3366596403971953291)
XLA Ops:
  7.2 0.0 copy-start
  7.2 0.0 all-gather.3.cloned.1.call-start
  7.2 0.8 fusion.151
  8.1 0.2 select_reduce_fusion.1
  8.3 0.0 copy-start.5
  8.3 1.4 convolution_convert_fusion.1
  9.7 32.9 %all_to_all.25 = bf16[8,128,512]{2,1,0:T(8,128)(2,1)} all-to-all(bf16[8,128,512]{2,1,0:T(8,128)(2,1)S(1)} %bitcast.122), channel_id=1, replica_groups=mesh['sp'=8,'tp'=4] {'sp'}, dimensions={0} | all-to-all | bytes 2097152 | tf_op jit(solution)/shard_map/all_to_all | solution.py:101
  42.7 0.0 all-gather.3.cloned.1.call-update
  42.7 0.0 copy-done.5
  42.7 0.3 add_reduce_fusion
  43.0 1.4 multiply_convert_fusion.1
  44.4 29.0 %all_to_all.26 = bf16[8,128,512]{2,1,0:T(8,128)(2,1)} all-to-all(bf16[8,128,512]{2,1,0:T(8,128)(2,1)S(1)} %bitcast.121), channel_id=1, replica_groups=mesh['sp'=8,'tp'=4] {'sp'}, dimensions={0} | all-to-all | bytes 2097152 | tf_op jit(solution)/shard_map/all_to_all | solution.py:104
  73.4 1.7 copy.20
  75.1 2.6 stack.2
  77.7 4.8 %all-to-all-start.2 = ((bf16[4,8,128,512]{2,1,3,0:T(8,128)(2,1)}), bf16[4,8,128,512]{2,1,3,0:T(8,128)(2,1)}, u32[]{:S(2)}, u32[]{:S(2)}) async-start(bf16[4,8,128,512]{2,1,3,0:T(8,128)(2,1)} %stack.2), calls=%async_computation.2 | async-start | bytes 8388608 | tf_op jit(solution)/shard_map/all_to_all | solution.py:109
  82.5 0.2 reduce-scatter.2.cloned.1.call-start
  82.7 0.0 all-gather.3.cloned.1.call-done
  82.7 0.0 copy-start.6
  82.8 6.6 %fusion.10 = f32[1024,512]{1,0:T(8,128)} fusion(bf16[1024,2048]{1,0:T(8,128)(2,1)} %bitcast.129, bf16[1,2048,512]{2,1,0:T(8,128)(2,1)} %param.22), kind=kOutput, calls=%fused_computation.12 | convolution fusion | flops 2147483648 | bytes 8388608 | tf_op jit(solution)/shard_map/dot_general | solution.py:52
  89.4 0.0 copy-done
  89.4 0.0 copy-done.6
  89.4 3.7 %fusion.15 = f32[1024,512]{1,0:T(8,128)} fusion(bf16[1024,2048]{1,0:T(8,128)(2,1)S(1)} %bitcast.132, bf16[1,2048,512]{2,1,0:T(8,128)(2,1)S(1)} %copy-done), kind=kOutput, calls=%fused_computation.17 | convolution fusion | flops 2147483648 | bytes 8388608 | tf_op jit(solution)/shard_map/dot_general | solution.py:51
  93.1 37.6 %all-to-all-done.2 = bf16[4,8,128,512]{2,1,3,0:T(8,128)(2,1)} async-done(((bf16[4,8,128,512]{2,1,3,0:T(8,128)(2,1)}), bf16[4,8,128,512]{2,1,3,0:T(8,128)(2,1)}, u32[]{:S(2)}, u32[]{:S(2)}) %all-to-all-start.2) | async-done | bytes 4194336 | tf_op jit(solution)/shard_map/all_to_all | solution.py:109
  130.7 7.7 %select_convert_fusion = (bf16[1024,512]{1,0:T(8,128)(2,1)S(1)}, bf16[1024,512]{1,0:T(8,128)(2,1)S(1)}) fusion(f32[1024,512]{1,0:T(8,128)} %fusion.10, f32[1024,512]{1,0:T(8,128)} %fusion.15, bf16[1,512,2048]{2,1,0:T(8,128)(2,1)} %param.23, bf16[256,8,8,128]{3,2,1,0:T(8,128)(2,1)} %bitcast.50), kind=kOutput, calls=%fused_computation.20 | convolution fusion | flops 2159017984 | bytes 12582912 | tf_op jit(solution)/shard_map/dot_general | solution.py:24
  138.4 0.0 copy-start.10
  138.4 0.0 copy-start.9
  138.4 0.0 copy-start.7
  138.5 2.4 fusion.13
  140.8 0.0 copy-done.10
  140.8 0.0 copy-done.9
  140.9 0.0 copy-done.7
  140.9 4.4 %add_convert_fusion = bf16[1024,2048]{1,0:T(8,128)(2,1)} fusion(f32[1024,2048]{1,0:T(8,128)S(1)} %fusion.13, bf16[1024,512]{1,0:T(8,128)(2,1)S(1)} %get-tuple-element.19, bf16[1,2048,512]{2,1,0:T(8,128)(2,1)S(1)} %copy-done.7), kind=kOutput, calls=%fused_computation | convolution fusion | flops 2151677952 | bytes 15728640 | tf_op jit(solution)/shard_map/dot_general | solution.py:24
  145.2 0.0 reduce-scatter.2.cloned.1.call-update
  145.3 0.0 copy-start.2
  145.3 0.0 copy-start.4
  145.3 42.6 %reduce-scatter.2.cloned.1.call-done = bf16[1024,512]{1,0:T(8,128)(2,1)} async-done(((bf16[1024,2048]{1,0:T(8,128)(2,1)}), bf16[1024,512]{1,0:T(8,128)(2,1)}) %reduce-scatter.2.cloned.1.call-update) | async-done | bytes 1048592 | tf_op jit(solution)/shard_map/reduce_scatter | solution.py:123
  187.9 5.5 %all-to-all-start.3 = ((bf16[8,128,512]{2,1,0:T(8,128)(2,1)}), bf16[8,128,512]{2,1,0:T(8,128)(2,1)S(1)}, u32[]{:S(2)}, u32[]{:S(2)}) async-start(bf16[8,128,512]{2,1,0:T(8,128)(2,1)} %bitcast.119), calls=%async_computation.4 | async-start | bytes 2097152 | tf_op jit(solution)/shard_map/all_to_all | solution.py:126
  193.4 0.0 all-gather.5.cloned.1.call-start
  193.4 0.0 copy-done.2
  193.4 0.1 fusion.120
  193.6 6.2 %all-reduce.1 = (f32[256]{0:T(256)S(1)}, f32[256]{0:T(256)S(1)}) all-reduce(f32[256]{0:T(256)S(1)} %get-tuple-element.10, f32[256]{0:T(256)S(1)} %get-tuple-element.9), channel_id=1, replica_groups=mesh['sp'=8,'tp'=4] {'tp'}, use_global_device_ids=true, to_apply=%region_7.8 | all-reduce | flops 512 | bytes 4096 | tf_op jit(solution)/shard_map/psum | solution.py:139
  199.8 0.0 copy-done.4
  199.8 19.2 %all-to-all-done.3 = bf16[8,128,512]{2,1,0:T(8,128)(2,1)S(1)} async-done(((bf16[8,128,512]{2,1,0:T(8,128)(2,1)}), bf16[8,128,512]{2,1,0:T(8,128)(2,1)S(1)}, u32[]{:S(2)}, u32[]{:S(2)}) %all-to-all-start.3) | async-done | bytes 1048608 | tf_op jit(solution)/shard_map/all_to_all | solution.py:126
  219.0 2.1 fusion.17
  221.2 0.0 all-gather.5.cloned.1.call-update
  221.2 0.0 copy-start.11
  221.2 0.0 copy-start.12
  221.2 7.0 %convolution_bitcast_fusion = f32[1,2048,512]{2,1,0:T(8,128)} fusion(bf16[1024,2048]{1,0:T(8,128)(2,1)} %bitcast.130, bf16[1024,512]{1,0:T(8,128)(2,1)} %copy-done.9), kind=kOutput, calls=%fused_computation.8 | convolution fusion | flops 2147483648 | bytes 9437184 | tf_op jit(solution)/shard_map/dot_general | solution.py:18
  228.3 7.3 %fusion.6 = f32[1,512,2048]{2,1,0:T(8,128)} fusion(bf16[256,8,8,128]{3,2,1,0:T(8,128)(2,1)} %bitcast.50, f32[1024,512]{1,0:T(8,128)S(1)} %copy-done.12, f32[1024,512]{1,0:T(8,128)S(1)} %copy-done.11), kind=kOutput, calls=%fused_computation.7 | convolution fusion | flops 2152726528 | bytes 12582912 | tf_op jit(solution)/shard_map/dot_general | solution.py:18
  235.6 0.5 all-gather.5.cloned.1.call-done
  236.1 1.8 fusion.149
  237.9 5.9 %all-reduce = (f32[256]{0:T(256)S(1)}, f32[256]{0:T(256)S(1)}) all-reduce(f32[256]{0:T(256)S(1)} %get-tuple-element.8, f32[256]{0:T(256)S(1)} %get-tuple-element.7), channel_id=1, replica_groups=mesh['sp'=8,'tp'=4] {'tp'}, use_global_device_ids=true, to_apply=%region_11.12 | all-reduce | flops 512 | bytes 4096 | tf_op jit(solution)/shard_map/psum | solution.py:150
  243.8 2.6 convolution_convert_fusion
  246.4 5.7 %all-to-all-start.4 = ((bf16[8,256,128]{2,1,0:T(8,128)(2,1)}), bf16[8,256,128]{2,1,0:T(8,128)(2,1)S(1)}, u32[]{:S(2)}, u32[]{:S(2)}) async-start(bf16[8,256,128]{2,1,0:T(8,128)(2,1)} %bitcast.44), calls=%async_computation.5 | async-start | bytes 1048576 | tf_op jit(solution)/shard_map/all_to_all | solution.py:170
  252.0 0.2 fusion.133
  252.3 0.0 copy-start.1
  252.3 0.0 copy-start.3
  252.3 1.4 collective-permute-start
  253.7 6.9 %convolution_bitcast_fusion.1 = f32[1,2048,512]{2,1,0:T(8,128)} fusion(bf16[1024,2048]{1,0:T(8,128)(2,1)} %bitcast.131, bf16[1024,512]{1,0:T(8,128)(2,1)} %copy-done.10), kind=kOutput, calls=%fused_computation.9 | convolution fusion | flops 2147483648 | bytes 9437184 | tf_op jit(solution)/shard_map/dot_general | solution.py:18
  260.6 0.0 collective-permute-done
  260.6 1.1 multiply_convert_fusion.3
  261.7 0.7 multiply_convert_fusion.4
  262.3 4.1 %all-to-all-done.4 = bf16[8,256,128]{2,1,0:T(8,128)(2,1)S(1)} async-done(((bf16[8,256,128]{2,1,0:T(8,128)(2,1)}), bf16[8,256,128]{2,1,0:T(8,128)(2,1)S(1)}, u32[]{:S(2)}, u32[]{:S(2)}) %all-to-all-start.4) | async-done | bytes 524320 | tf_op jit(solution)/shard_map/all_to_all | solution.py:170
  266.4 0.7 convert_reduce_fusion
  (14 shorter events, 0.1 us)
Async XLA Ops:
  7.2 82.2 %copy-start = (bf16[1,2048,512]{2,1,0:T(8,128)(2,1)S(1)}, bf16[1,2048,512]{2,1,0:T(8,128)(2,1)}, u32[]{:S(2)}) copy-start(bf16[1,2048,512]{2,1,0:T(8,128)(2,1)} %param.21) | copy-start | bytes 6291460
  7.2 75.6 %all-gather.3.cloned.1.call-start = ((), (), s32[]{:S(2)}) async-start(), calls=%async_computation.6 | async-start | bytes 5242880 | tf_op jit(solution)/shard_map/all_gather | solution.py:107
  8.3 34.4 %copy-start.5 = (f32[256,2]{0,1:T(2,128)S(1)}, f32[256,2]{0,1:T(2,128)}, u32[]{:S(2)}) copy-start(f32[256,2]{0,1:T(2,128)} %param.15) | copy-start | bytes 6148
  77.7 53.0 %all-to-all-start.2 = ((bf16[4,8,128,512]{2,1,3,0:T(8,128)(2,1)}), bf16[4,8,128,512]{2,1,3,0:T(8,128)(2,1)}, u32[]{:S(2)}, u32[]{:S(2)}) async-start(bf16[4,8,128,512]{2,1,3,0:T(8,128)(2,1)} %stack.2), calls=%async_computation.2 | async-start | bytes 8388608 | tf_op jit(solution)/shard_map/all_to_all | solution.py:109
  82.5 105.4 %reduce-scatter.2.cloned.1.call-start = ((), (), s32[]{:S(2)}) async-start(), calls=%async_computation.7 | async-start | bytes 5242880 | tf_op jit(solution)/shard_map/reduce_scatter | solution.py:123
  82.7 6.7 %copy-start.6 = (bf16[8,128,2048]{2,1,0:T(8,128)(2,1)S(1)}, bf16[8,128,2048]{2,1,0:T(8,128)(2,1)}, u32[]{:S(2)}) copy-start(bf16[8,128,2048]{2,1,0:T(8,128)(2,1)} %all-gather.3.cloned.1.call-done) | copy-start | bytes 12582916
  138.4 2.4 copy-start.10
  138.4 2.4 copy-start.9
  138.4 2.4 copy-start.7
  145.3 48.2 %copy-start.2 = (bf16[256,128]{1,0:T(8,128)(2,1)S(1)}, bf16[256,128]{1,0:T(8,128)(2,1)}, u32[]{:S(2)}) copy-start(bf16[256,128]{1,0:T(8,128)(2,1)} %param.19) | copy-start | bytes 196612
  145.3 54.5 %copy-start.4 = (f32[31,128]{1,0:T(8,128)S(1)}, f32[31,128]{1,0:T(8,128)}, u32[]{:S(2)}) copy-start(f32[31,128]{1,0:T(8,128)} %param.18) | copy-start | bytes 47620
  187.9 31.2 %all-to-all-start.3 = ((bf16[8,128,512]{2,1,0:T(8,128)(2,1)}), bf16[8,128,512]{2,1,0:T(8,128)(2,1)S(1)}, u32[]{:S(2)}, u32[]{:S(2)}) async-start(bf16[8,128,512]{2,1,0:T(8,128)(2,1)} %bitcast.119), calls=%async_computation.4 | async-start | bytes 2097152 | tf_op jit(solution)/shard_map/all_to_all | solution.py:126
  193.4 42.7 %all-gather.5.cloned.1.call-start = ((), (), s32[]{:S(2)}) async-start(), calls=%async_computation.8 | async-start | bytes 1310720 | tf_op jit(solution)/shard_map/all_gather | solution.py:136
  221.2 7.1 %copy-start.11 = (f32[1024,512]{1,0:T(8,128)S(1)}, f32[1024,512]{1,0:T(8,128)}, u32[]{:S(2)}) copy-start(f32[1024,512]{1,0:T(8,128)} %fusion.10) | copy-start | bytes 6291460
  221.2 7.0 %copy-start.12 = (f32[1024,512]{1,0:T(8,128)S(1)}, f32[1024,512]{1,0:T(8,128)}, u32[]{:S(2)}) copy-start(f32[1024,512]{1,0:T(8,128)} %fusion.15) | copy-start | bytes 6291460
  228.3 7.8 %copy-start.8 = (bf16[2048,128]{1,0:T(8,128)(2,1)S(1)}, bf16[2048,128]{1,0:T(8,128)(2,1)}, u32[]{:S(2)}) copy-start(bf16[2048,128]{1,0:T(8,128)(2,1)} %param.20) | copy-start | bytes 1572868
  246.4 20.0 %all-to-all-start.4 = ((bf16[8,256,128]{2,1,0:T(8,128)(2,1)}), bf16[8,256,128]{2,1,0:T(8,128)(2,1)S(1)}, u32[]{:S(2)}, u32[]{:S(2)}) async-start(bf16[8,256,128]{2,1,0:T(8,128)(2,1)} %bitcast.44), calls=%async_computation.5 | async-start | bytes 1048576 | tf_op jit(solution)/shard_map/all_to_all | solution.py:170
  252.3 8.3 %copy-start.1 = (bf16[256,128]{1,0:T(8,128)(2,1)S(1)}, bf16[256,128]{1,0:T(8,128)(2,1)}, u32[]{:S(2)}) copy-start(bf16[256,128]{1,0:T(8,128)(2,1)} %param.17) | copy-start | bytes 196612
  252.3 8.3 %copy-start.3 = (bf16[256,128]{1,0:T(8,128)(2,1)S(1)}, bf16[256,128]{1,0:T(8,128)(2,1)}, u32[]{:S(2)}) copy-start(bf16[256,128]{1,0:T(8,128)(2,1)} %param.16) | copy-start | bytes 196612
  252.3 8.3 %collective-permute-start = (f32[30,128]{1,0:T(8,128)S(1)}, f32[30,128]{1,0:T(8,128)S(1)}, u32[]{:S(2)}, u32[]{:S(2)}) collective-permute-start(f32[30,128]{1,0:T(8,128)S(1)} %slice.266), channel_id=1, source_target_pairs={{4,0},{8,4},{12,8},{16,12},{20,16},{24,20},{28,24},{5,1},{9,5},{13... | collective-permute-start | bytes 46088 | tf_op jit(solution)/shard_map/ppermute | solution.py:14
Sparse Core Ops, SparseCore 0:
  42.8 33.4 all-gather.2
  145.4 42.4 reduce-scatter.1
  221.3 14.7 all-gather.4
